TPU v7x, 256 devices: a whole 4x4x8 slice. The times are simulated.
256 devices in a mesh: fs: 64 (over z, x, core), tp: 4 (over y).
Axes of the slice: x: 4, y: 4, z: 8, core: 2. Of those that a mesh axis runs over, the one named last changes fastest.
Arguments:
- tokens: bfloat16 [768, 4, 2048], P(None, 'tp'), may hold values from -6 to 6
- norm_gain: float32 [2048], P('fs'), may hold values from 0.1 to 1.9
- gate_weight: float32 [8, 2048, 4096], P(None, 'fs', 'tp'), may hold values from -0.125 to 0.125
- up_weight: float32 [8, 2048, 4096], P(None, 'fs', 'tp'), may hold values from -0.125 to 0.125
- down_weight: float32 [8, 2048, 4096], P(None, 'fs', 'tp'), may hold values from -0.09375 to 0.09375
- expert_ids: int32 [768, 4, 2], P(None, 'tp'), may hold values from 0 to 7, all different within a row
- expert_mix: float32 [768, 4, 2], P(None, 'tp'), may hold values from 0.2 to 1
Outputs:
- gate_serve: bfloat16 [8, 2048, 4096], P(None, None, 'fs')
- up_serve: bfloat16 [8, 2048, 4096], P(None, None, 'fs')
- down_serve: bfloat16 [8, 2048, 4096], P(None, None, 'fs')
- mixed: bfloat16 [768, 4, 2048], P('fs', 'tp')
Inputs may be any that keep to these rules, and one draw needn't show every extreme that they name: `expert_ids`: each token names two different experts.
All inputs are finite; a program needn't handle non-finite values.
Results may differ from a plain program's by a relative error of at most 0.0082.
Values may be sent and summed in bfloat16 or wider, within the bound.
A program may use at most 64 MiB of HBM per device.

v0:
```python
import jax
import jax.numpy as jnp
from jax import lax
from jax.sharding import Mesh
from jax.sharding import PartitionSpec as P

FS = ("fs_0", "fs_1", "fs_2")


norm_eps = 1e-05


def sent_together(arrays, axis, split_dim, concat_dim, along):
    ends, at = ([], 0)
    for a in arrays[:-1]:
        at += a.shape[along]
        ends.append(at)
    both = jnp.concatenate(arrays, axis=along)
    return tuple(
        jnp.split(
            lax.all_to_all(both, axis, split_axis=split_dim, concat_axis=concat_dim, tiled=True),
            ends,
            axis=along,
        )
    )


def sent_together_2(arrays, axis, dim, along):
    both = jnp.concatenate(arrays, axis=along)
    result, at, gathered = (lax.all_gather(both, axis, axis=dim, tiled=True), 0, [])
    for a in arrays:
        gathered.append(lax.slice_in_dim(result, at, at + a.shape[along], axis=along))
        at += a.shape[along]
    return tuple(gathered)


def summed_rows(so_far, axes):
    for axis in axes:
        so_far = lax.psum_scatter(so_far, axis, scatter_dimension=0, tiled=True)
    return so_far


def local(tokens, norm_gain, gate_weight, up_weight, down_weight, expert_ids, expert_mix):
    gate_folded = (gate_weight * norm_gain[None, :, None]).astype(jnp.bfloat16)
    up_folded = (up_weight * norm_gain[None, :, None]).astype(jnp.bfloat16)
    down_cast = down_weight.astype(jnp.bfloat16)
    regrouped = sent_together((gate_folded, up_folded, down_cast), "tp", 0, 2, 1)
    unit_split = sent_together((regrouped[0], regrouped[1], regrouped[2]), FS, 2, 1, 0)
    gate_serve, up_serve, down_serve = sent_together_2(
        (unit_split[0], unit_split[1], unit_split[2]), "tp", 0, 1
    )
    width = tokens.shape[2]
    token_rows = tokens.reshape(-1, width).astype(jnp.float32)
    row_mean = jnp.mean(token_rows, axis=1, keepdims=True)
    centered = token_rows - row_mean
    variance = jnp.mean(centered * centered, axis=1, keepdims=True)
    normed = (centered * lax.rsqrt(variance + norm_eps)).astype(jnp.bfloat16)
    route_ids = expert_ids.reshape(-1, 2)
    route_mix = expert_mix.reshape(-1, 2)
    expert_iota = jnp.arange(gate_serve.shape[0], dtype=jnp.int32)
    expert_gates = jnp.sum(
        (route_ids[:, :, None] == expert_iota[None, None, :]).astype(jnp.float32)
        * route_mix[:, :, None],
        axis=1,
    )
    gate_act = jnp.einsum("rd,edf->ref", normed, gate_serve, preferred_element_type=jnp.float32)
    up_act = jnp.einsum("rd,edf->ref", normed, up_serve, preferred_element_type=jnp.float32)
    hidden = (jax.nn.silu(gate_act) * up_act * expert_gates[:, :, None]).astype(jnp.bfloat16)
    own_rows = token_rows.shape[0] // lax.axis_size(FS)
    summed = summed_rows(
        jnp.einsum("ref,edf->rd", hidden, down_serve, preferred_element_type=jnp.float32), FS
    )
    mixed = summed.astype(jnp.bfloat16).reshape(own_rows, 1, width)
    return (gate_serve, up_serve, down_serve, mixed)


def solution(mesh):
    finer = Mesh(mesh.devices.reshape(8, 4, 2, mesh.shape["tp"]), ("fs_0", "fs_1", "fs_2", "tp"))
    placed = (
        P(None, "tp", None),
        P(FS),
        P(None, FS, "tp"),
        P(None, FS, "tp"),
        P(None, FS, "tp"),
        P(None, "tp", None),
        P(None, "tp", None),
    )
    return jax.shard_map(
        local,
        mesh=finer,
        in_specs=placed,
        out_specs=(P(None, None, FS), P(None, None, FS), P(None, None, FS), P(FS, "tp", None)),
        check_vma=False,
    )
```

profile of v0, /device:TPU:1, one launch (start us, length us, event | category | flops | bytes accessed | tf_op | source)
XLA Modules:
  0.0 326.5 jit_solution(13660195549617188783)
XLA Ops:
  7.2 1.4 convert_element_type.27
  8.7 1.5 multiply_convert_fusion.2
  10.4 24.7 %all_to_all.33 = bf16[8,96,1024]{2,1,0:T(8,128)(2,1)S(1)} all-to-all(bf16[8,96,1024]{2,1,0:T(8,128)(2,1)S(1)} %pad_maximum_fusion.1), channel_id=1, replica_groups=mesh['fs_0'=8,'fs_1'=4,'fs_2'=2,'tp'=4] {'tp'}, dimensions={0} | all-to-all | bytes 3145728 | tf_op jit(solution)/shard_map/all_to_all | solution.py:21
  35.0 1.2 copy.40
  36.3 1.2 all_to_all.27
  37.8 7.3 %copy.32 = bf16[6,32,4096]{1,0,2:T(8,128)(2,1)} copy(bf16[6,32,4096]{2,1,0:T(8,128)(2,1)S(1)} %pad_maximum_fusion.2) | data formatting | bytes 3145728 | tf_op jit(solution)/shard_map/concatenate | solution.py:18
  45.1 10.7 %reshape.39 = bf16[64,2,6144]{2,1,0:T(2,128)(2,1)S(1)} reshape(bf16[4096,6,32]{2,1,0:T(8,128)(2,1)} %bitcast.45) | data formatting | bytes 3145728
  55.8 52.1 %all_to_all.34 = bf16[64,2,6144]{2,1,0:T(2,128)(2,1)S(1)} all-to-all(bf16[64,2,6144]{2,1,0:T(2,128)(2,1)S(1)} %reshape.39), channel_id=1, replica_groups=mesh['fs_0'=8,'fs_1'=4,'fs_2'=2,'tp'=4] {'fs_0','fs_1','fs_2'}, dimensions={0} | all-to-all | bytes 3145728 | tf_op jit(solution)/shard_map/all_to_all | solution.py:21
  108.0 7.6 %reshape.40 = bf16[4096,6,32]{2,1,0:T(8,128)(2,1)} reshape(bf16[64,2,6144]{2,1,0:T(2,128)(2,1)S(1)} %all_to_all.34) | data formatting | bytes 3145728
  115.5 8.6 %copy.38 = bf16[6,32,64,64]{3,2,1,0:T(8,128)(2,1)S(1)} copy(bf16[6,32,64,64]{1,0,3,2:T(8,128)(2,1)} %bitcast.46) | data formatting | bytes 3145728 | tf_op jit(solution)/shard_map/all_to_all | solution.py:21
  124.1 0.7 fusion.15
  124.8 0.7 copy.34
  126.9 2.0 pad_maximum_fusion
  128.9 4.4 %copy.37 = bf16[2,6144,64]{1,2,0:T(8,128)(2,1)} copy(bf16[2,6144,64]{2,1,0:T(8,128)(2,1)} %pad_maximum_fusion) | data formatting | bytes 3145728 | tf_op jit(solution)/shard_map/concatenate | solution.py:29
  134.1 1.0 fusion.4
  135.0 61.6 %all-gather.2.cloned.1.call-done = bf16[8,6144,64]{1,2,0:T(8,128)(2,1)} async-done(((bf16[2,6144,64]{1,2,0:T(8,128)(2,1)}), bf16[8,6144,64]{1,2,0:T(8,128)(2,1)}) %all-gather.2.cloned.1.call-update) | async-done | bytes 6291472 | tf_op jit(solution)/shard_map/all_gather | solution.py:30
  196.7 4.0 %fusion.14 = (bf16[8,2048,64]{1,2,0:T(8,128)(2,1)S(1)}, bf16[8,2048,64]{1,2,0:T(8,128)(2,1)S(1)}, bf16[8,2048,64]{1,2,0:T(8,128)(2,1)S(1)}) fusion(bf16[8,6144,64]{1,2,0:T(8,128)(2,1)} %all-gather.2.cloned.1.call-done), kind=kLoop, calls=%fused_computation.26 | loop fusion | bytes 12582912 | tf_op jit(solution)/shard_map/slice | solution.py:32
  200.7 1.9 fusion.12
  202.7 1.9 fusion.10
  204.6 4.6 %convolution_bitcast_fusion = f32[768,2048]{1,0:T(8,128)} fusion(bf16[8,2048,64]{1,2,0:T(8,128)(2,1)S(1)} %get-tuple-element.4, f32[768,8,64]{0,2,1:T(8,128)S(1)} %bitcast.58, f32[768,8,64]{0,2,1:T(8,128)S(1)} %bitcast.57, f32[768,8]{0,1:T(8,128)S(1)} %select_reduce_fusion), kind=kOutput, calls=%fused_computation.7 | convolution fusion | flops 1613365248 | bytes 11558912 | tf_op jit(solution)/shard_map/ref,edf->rd/dot_general | solution.py:71
  209.2 76.0 %reduce-scatter.5.cloned.1.call-done = f32[96,2048]{1,0:T(8,128)} async-done(((f32[768,2048]{1,0:T(8,128)}), f32[96,2048]{1,0:T(8,128)}) %reduce-scatter.5.cloned.1.call-update) | async-done | bytes 786448 | tf_op jit(solution)/shard_map/reduce_scatter | solution.py:39
  285.3 24.2 %reduce-scatter.7.cloned.1.call-done = f32[24,2048]{1,0:T(8,128)} async-done(((f32[96,2048]{1,0:T(8,128)}), f32[24,2048]{1,0:T(8,128)}) %reduce-scatter.7.cloned.1.call-update) | async-done | bytes 196624 | tf_op jit(solution)/shard_map/reduce_scatter | solution.py:39
  309.5 6.5 %fusion = f32[16,2048]{1,0:T(8,128)S(1)} fusion(f32[24,2048]{1,0:T(8,128)} %reduce-scatter.7.cloned.1.call-done), kind=kCustom, calls=%all-reduce-scatter | all-reduce-scatter fusion | flops 65537 | bytes 328704
  316.0 1.3 collective-permute-start
  (36 shorter events, 4.8 us)
Async XLA Ops:
  7.2 1.5 copy-start.4
  7.2 189.5 %all-gather.2.cloned.1.call-start = ((), (), s32[]{:S(2)}) async-start(), calls=%async_computation.4 | async-start | bytes 7864320 | tf_op jit(solution)/shard_map/all_gather | solution.py:30
  128.8 4.7 %copy-start.5 = (f32[768,1,2]{0,2,1:T(2,128)S(1)}, f32[768,1,2]{0,2,1:T(2,128)}, u32[]{:S(2)}) copy-start(f32[768,1,2]{0,2,1:T(2,128)} %param.13) | copy-start | bytes 18436
  128.8 4.7 %copy-start.6 = (s32[768,1,2]{0,2,1:T(2,128)S(1)}, s32[768,1,2]{0,2,1:T(2,128)}, u32[]{:S(2)}) copy-start(s32[768,1,2]{0,2,1:T(2,128)} %param.12) | copy-start | bytes 18436
  128.8 4.7 %copy-start = (bf16[768,1,2048]{2,0,1:T(8,128)(2,1)S(1)}, bf16[768,1,2048]{2,0,1:T(8,128)(2,1)}, u32[]{:S(2)}) copy-start(bf16[768,1,2048]{2,0,1:T(8,128)(2,1)} %param.7) | copy-start | bytes 9437188
  133.3 151.9 %reduce-scatter.5.cloned.1.call-start = ((), (), s32[]{:S(2)}) async-start(), calls=%async_computation.5 | async-start | bytes 7077888 | tf_op jit(solution)/shard_map/reduce_scatter | solution.py:39
  200.7 1.9 copy-start.3
  200.7 2.0 copy-start.2
  200.7 3.9 %copy-start.1 = (bf16[8,2048,64]{1,2,0:T(8,128)(2,1)}, bf16[8,2048,64]{1,2,0:T(8,128)(2,1)S(1)}, u32[]{:S(2)}) copy-start(bf16[8,2048,64]{1,2,0:T(8,128)(2,1)S(1)} %get-tuple-element.4) | copy-start | bytes 6291460
  209.2 108.1 %copy-start.7 = (u32[256]{0:T(256)S(1)}, u32[256]{0:T(256)}, u32[]{:S(2)}) copy-start(u32[256]{0:T(256)} %constant.21) | copy-start | bytes 3076
  209.2 100.3 %reduce-scatter.7.cloned.1.call-start = ((), (), s32[]{:S(2)}) async-start(), calls=%async_computation.6 | async-start | bytes 983040 | tf_op jit(solution)/shard_map/reduce_scatter | solution.py:39
  316.0 3.1 collective-permute-start
Sparse Core Ops, SparseCore 0:
  133.4 63.2 all-gather.1
  209.3 75.8 reduce-scatter.4
  287.8 21.6 reduce-scatter.6
where the time goes:
time: 327 us; the launch traced here: 326 us
  waiting for transfers between devices  162 us (50%)
  blocking collectives  83.3 us (25%)
  local copies, waits for them, and re-layouts  49.5 us (15%)
  between operations  14.6 us (4%)
  matrix products  8.38 us (3%)
  other arithmetic  6.63 us (2%)
    reduce_scatter x2, waiting for transfers between devices, summed_rows(): so_far = lax.psum_scatter(so_far, axis, scatter_dimension=0, tiled=True)  100 us
    all_to_all x2, blocking collectives, sent_together(): lax.all_to_all(both, axis, split_axis=split_dim, concat_axis=concat_dim,...  76.8 us
    all_gather x1, waiting for transfers between devices, sent_together_2(): lax.all_gather(both, axis, axis=dim, tiled=True)  61.6 us
    unnamed x21, local copies, waits for them, and re-layouts  19.3 us
    all_to_all x3, local copies, waits for them, and re-layouts, sent_together(): lax.all_to_all(both, axis, split_axis=split_dim, concat_axis=concat_dim,...  11 us
    concatenate x1, local copies, waits for them, and re-layouts, sent_together(): both = jnp.concatenate(arrays, axis=along)  7.33 us
  transfers between devices with their start and end apart: 4, of which 4 were waited for; matrix products, arithmetic and copies ran while one was open for 1% of the time, Pallas kernels for 0%

commit v1 on v0

v1 whole, which is shorter than its diff:
```python
import functools

import jax
import jax.numpy as jnp
from jax import lax
from jax.experimental import pallas as pl
from jax.experimental.pallas import tpu as pltpu
from jax.sharding import Mesh
from jax.sharding import PartitionSpec as P

FS = ("fs_0", "fs_1", "fs_2")
NZ, NX, NC, NY = 8, 4, 2, 4
NXC = NX * NC
MESH = pl.DeviceIdType.MESH


norm_eps = 1e-05


def remote(src, dst, send, recv, **where):
    return pltpu.make_async_remote_copy(
        src_ref=src, dst_ref=dst, send_sem=send, recv_sem=recv, device_id=where, device_id_type=MESH
    )


def greet(peers):
    barrier = pltpu.get_barrier_semaphore()
    for where in peers:
        pl.semaphore_signal(barrier, inc=1, device_id=where, device_id_type=MESH)
    pl.semaphore_wait(barrier, len(peers))


def weights_kernel(
    gain_ref, gate_hbm, up_hbm, down_hbm, gate_out, up_out, down_out,
    win, packed, by_plane, by_z, rows, turned,
    in_sem, out_sem, y_send, y_recv, z_send, z_recv, x_send, x_recv, g_send, g_recv,
):
    z, x, c, y = (lax.axis_index(a) for a in ("fs_0", "fs_1", "fs_2", "tp"))
    xc = x * NC + c
    loads = [
        pltpu.make_async_copy(ref, win.at[w], in_sem.at[w])
        for w, ref in enumerate((gate_hbm, up_hbm, down_hbm))
    ]
    for load in loads:
        load.start()

    def z_of(j):
        return lax.rem(z + j, NZ)

    def y_of(j):
        return lax.rem(y + j, NY)

    def xc_of(j):
        to = lax.rem(xc + j, NXC)
        return to, {"fs_1": lax.div(to, NC), "fs_2": lax.rem(to, NC)}

    greet(
        [{"tp": y_of(j)} for j in range(1, NY)]
        + [{"fs_0": z_of(j)} for j in range(1, NZ)]
        + [xc_of(j)[1] for j in range(1, NXC)]
    )

    sent = []

    def go(copy):
        copy.start()
        sent.append(copy)
        return copy

    left_lanes = lax.broadcasted_iota(jnp.int32, (32, 128), 1) < 64

    def fold(w):
        loads[w].wait()

        def block(j, carry):
            at = pl.ds(pl.multiple_of(j * 128, 128), 128)
            for g in range(NY):
                one = win[w, 2 * g, :, at]
                two = win[w, 2 * g + 1, :, at]
                if w < 2:
                    one, two = one * gain_ref[...], two * gain_ref[...]
                first = jnp.where(left_lanes, one, pltpu.roll(two, 64, 1))
                second = jnp.where(left_lanes, pltpu.roll(one, 64, 1), two)
                packed[w, g, 2 * j] = first.astype(jnp.bfloat16)
                packed[w, g, 2 * j + 1] = second.astype(jnp.bfloat16)
            return carry

        lax.fori_loop(0, 8, block, 0)

    def y_copies(w):
        return [
            remote(
                packed.at[w, y_of(j)], by_plane.at[w, y],
                y_send.at[w, j - 1], y_recv.at[w, j - 1], tp=y_of(j),
            )
            for j in (1, 3, 2)
        ]

    def z_copies(w):
        copies = []
        for j in (1, 7, 2, 6, 3, 5, 4):
            to = z_of(j)
            half = lax.rem(to, 2) * 8
            copies.append(
                remote(
                    by_plane.at[w, lax.div(to, 2), pl.ds(half, 8)], by_z.at[w, z],
                    z_send.at[w, j - 1], z_recv.at[w, j - 1], fs_0=to,
                )
            )
        return copies

    def x_copies(w):
        copies = []
        for j in range(1, NXC):
            to, where = xc_of(j)
            copies.append(
                remote(
                    by_z.at[w, :, to], rows.at[w, y, :, xc],
                    x_send.at[w, j - 1], x_recv.at[w, j - 1], **where,
                )
            )
        return copies

    def g_copies(w):
        return [
            remote(rows.at[w, y], rows.at[w, y], g_send.at[w, 0], g_recv.at[w, 0], tp=y_of(1)),
            remote(rows.at[w, y], rows.at[w, y], g_send.at[w, 1], g_recv.at[w, 1], tp=y_of(3)),
        ]

    def f_copies(w):
        lo = rows.at[w, y_of(3), pl.ds(0, 4)]
        hi = rows.at[w, y_of(1), pl.ds(4, 4)]
        return [
            remote(lo, lo, g_send.at[w, 2], g_recv.at[w, 2], tp=y_of(1)),
            remote(hi, hi, g_send.at[w, 3], g_recv.at[w, 3], tp=y_of(3)),
        ]

    ys, zs, xs, gs, fs = ([None] * 3 for _ in range(5))

    def wait(copies):
        for copy in copies:
            copy.wait_recv()

    def start_y(w):
        fold(w)
        ys[w] = [go(copy) for copy in y_copies(w)]
        by_plane[w, y] = packed[w, y]

    def start_z(w):
        wait(ys[w])
        zs[w] = [go(copy) for copy in z_copies(w)]
        by_z[w, z] = by_plane[w, lax.div(z, 2), pl.ds(lax.rem(z, 2) * 8, 8)]

    def start_x(w):
        wait(zs[w])
        xs[w] = [go(copy) for copy in x_copies(w)]
        rows[w, y, :, xc] = by_z[w, :, xc]

    def start_g(w):
        wait(xs[w])
        gs[w] = [go(copy) for copy in g_copies(w)]

    def start_f(w):
        wait(gs[w])
        fs[w] = [go(copy) for copy in f_copies(w)]

    def turn(w, g):
        def block(i, carry):
            tile = rows[w, g, lax.div(i, 2), pl.ds(lax.rem(i, 2) * 4, 4)]
            tile = tile.reshape(128, 128).astype(jnp.float32).T.astype(jnp.bfloat16)
            at = pl.ds(pl.multiple_of(i * 128, 128), 128)
            turned[w, g, :, at] = tile
            return carry

        lax.fori_loop(0, 16, block, 0)

    outs = (gate_out, up_out, down_out)
    stores = []

    def finish(w):
        wait(fs[w])
        turn(w, y_of(2))
        store = pltpu.make_async_copy(turned.at[w], outs[w], out_sem.at[w])
        store.start()
        stores.append(store)

    start_y(0)
    start_y(1)
    start_y(2)
    start_z(0)
    start_z(1)
    start_z(2)
    start_x(0)
    start_g(0)
    start_x(1)
    turn(0, y)
    start_g(1)
    start_f(0)
    start_x(2)
    turn(1, y)
    turn(0, y_of(1))
    turn(0, y_of(3))
    start_g(2)
    start_f(1)
    finish(0)
    turn(1, y_of(1))
    turn(1, y_of(3))
    turn(2, y)
    start_f(2)
    finish(1)
    turn(2, y_of(1))
    turn(2, y_of(3))
    finish(2)
    for copy in sent:
        copy.wait_send()
    for store in stores:
        store.wait()


def handed_over(norm_gain, gate_weight, up_weight, down_weight):
    bf16, dma = jnp.bfloat16, pltpu.SemaphoreType.DMA
    out = jax.ShapeDtypeStruct((NY, 128, 2048), bf16)
    anywhere = pl.BlockSpec(memory_space=pl.ANY)
    gain = jnp.broadcast_to(norm_gain[:, None], (32, 128))
    return pl.pallas_call(
        weights_kernel,
        out_shape=(out, out, out),
        in_specs=[pl.BlockSpec(memory_space=pltpu.VMEM), anywhere, anywhere, anywhere],
        out_specs=(anywhere, anywhere, anywhere),
        scratch_shapes=[
            pltpu.VMEM((3, 8, 32, 1024), jnp.float32),
            pltpu.VMEM((3, NY, 16, 32, 128), bf16),
            pltpu.VMEM((3, NY, 16, 32, 128), bf16),
            pltpu.VMEM((3, NZ, NXC, 32, 128), bf16),
            pltpu.VMEM((3, NY, NZ, NXC, 32, 128), bf16),
            pltpu.VMEM((3, NY, 128, 2048), bf16),
            dma((3,)), dma((3,)),
            dma((3, 3)), dma((3, 3)),
            dma((3, 7)), dma((3, 7)),
            dma((3, 7)), dma((3, 7)),
            dma((3, 4)), dma((3, 4)),
        ],
        compiler_params=pltpu.CompilerParams(
            collective_id=0, has_side_effects=True, vmem_limit_bytes=56 * 2**20
        ),
        name="weights",
    )(gain, gate_weight, up_weight, down_weight)


def sum_kernel(
    part, out_ref, pair_in, chip, xa_in, xb_in, mine, z_in, piece, other,
    p_send, p_recv, x_send, x_recv, z_send, z_recv, o_send, o_recv,
):
    z, x, c = (lax.axis_index(a) for a in FS)
    f32, bf16 = jnp.float32, jnp.bfloat16
    right, left, far = (lax.rem(x + j, NX) for j in (1, 3, 2))

    def z_of(j):
        return lax.rem(z + j, NZ)

    greet(
        [{"fs_2": 1 - c}, {"fs_1": right}, {"fs_1": left}]
        + [{"fs_0": z_of(j)} for j in range(1, NZ)]
    )
    sent = []

    def go(copy):
        copy.start()
        sent.append(copy)
        return copy

    def columns(of):
        return pl.ds(pl.multiple_of(of * 1024, 1024), 1024)

    pair = go(remote(part.at[:, :, :, columns(1 - c)], pair_in, p_send, p_recv, fs_2=1 - c))
    pair.wait_recv()

    def add_pair(i, carry):
        for j in range(NX):
            own = part[i, j, :, columns(c)].astype(f32)
            chip[i, j] = (own + pair_in[i, j].astype(f32)).astype(bf16)
        return carry

    lax.fori_loop(0, NZ, add_pair, 0)
    lo, hi = pl.ds(0, 4), pl.ds(4, 4)
    far_r = go(remote(chip.at[lo, far], xa_in.at[0], x_send.at[0], x_recv.at[0], fs_1=right))
    far_l = go(remote(chip.at[hi, far], xb_in.at[0], x_send.at[1], x_recv.at[1], fs_1=left))
    own_r = go(remote(chip.at[hi, right], xa_in.at[2], x_send.at[2], x_recv.at[2], fs_1=right))
    own_l = go(remote(chip.at[lo, left], xb_in.at[2], x_send.at[3], x_recv.at[3], fs_1=left))

    def add_far(start, to, got):
        def step(i, carry):
            chip[start + i, to] = (
                chip[start + i, to].astype(f32) + got[0, i].astype(f32)
            ).astype(bf16)
            return carry

        lax.fori_loop(0, 4, step, 0)

    far_r.wait_recv()
    add_far(0, right, xa_in)
    sum_r = go(remote(chip.at[lo, right], xa_in.at[1], x_send.at[4], x_recv.at[4], fs_1=right))
    far_l.wait_recv()
    add_far(4, left, xb_in)
    sum_l = go(remote(chip.at[hi, left], xb_in.at[1], x_send.at[5], x_recv.at[5], fs_1=left))
    own_r.wait_recv()
    own_l.wait_recv()
    sum_r.wait_recv()
    sum_l.wait_recv()

    def add_x(i, carry):
        mine[i] = (
            chip[i, x].astype(f32) + xa_in[1, i].astype(f32) + xb_in[2, i].astype(f32)
        ).astype(bf16)
        mine[4 + i] = (
            chip[4 + i, x].astype(f32) + xa_in[2, i].astype(f32) + xb_in[1, i].astype(f32)
        ).astype(bf16)
        return carry

    lax.fori_loop(0, 4, add_x, 0)
    zs = [
        go(remote(mine.at[z_of(j)], z_in.at[j - 1], z_send.at[j - 1], z_recv.at[j - 1], fs_0=z_of(j)))
        for j in (1, 7, 2, 6, 3, 5, 4)
    ]
    for copy in zs:
        copy.wait_recv()
    total = mine[z].astype(f32)
    for j in range(7):
        total = total + z_in[j].astype(f32)
    piece[...] = total.astype(bf16)
    last = go(remote(piece, other, o_send, o_recv, fs_2=1 - c))
    last.wait_recv()
    here, there = piece[...].astype(f32), other[...].astype(f32)
    here = jnp.where(c == 0, here[:12], here[12:])
    there = jnp.where(c == 0, there[:12], there[12:])
    out_ref[:, :1024] = jnp.where(c == 0, here, there).astype(bf16)
    out_ref[:, 1024:] = jnp.where(c == 0, there, here).astype(bf16)
    for copy in sent:
        copy.wait_send()


def summed_rows(part):
    bf16, dma = jnp.bfloat16, pltpu.SemaphoreType.DMA
    return pl.pallas_call(
        sum_kernel,
        out_shape=jax.ShapeDtypeStruct((12, 2048), bf16),
        in_specs=[pl.BlockSpec(memory_space=pltpu.VMEM)],
        out_specs=pl.BlockSpec(memory_space=pltpu.VMEM),
        scratch_shapes=[
            pltpu.VMEM((NZ, NX, 24, 1024), bf16),
            pltpu.VMEM((NZ, NX, 24, 1024), bf16),
            pltpu.VMEM((3, 4, 24, 1024), bf16),
            pltpu.VMEM((3, 4, 24, 1024), bf16),
            pltpu.VMEM((NZ, 24, 1024), bf16),
            pltpu.VMEM((7, 24, 1024), bf16),
            pltpu.VMEM((24, 1024), bf16),
            pltpu.VMEM((24, 1024), bf16),
            dma, dma, dma((6,)), dma((6,)), dma((7,)), dma((7,)), dma, dma,
        ],
        compiler_params=pltpu.CompilerParams(
            collective_id=1, has_side_effects=True, vmem_limit_bytes=40 * 2**20
        ),
        name="sums",
    )(part.reshape(NZ, NX, 24, 2048))


def local(tokens, norm_gain, gate_weight, up_weight, down_weight, expert_ids, expert_mix):
    gate_serve, up_serve, down_serve = (
        jnp.swapaxes(a.reshape(8, 64, 2048), 1, 2)
        for a in handed_over(norm_gain, gate_weight, up_weight, down_weight)
    )
    width = tokens.shape[2]
    token_rows = tokens.reshape(-1, width).astype(jnp.float32)
    row_mean = jnp.mean(token_rows, axis=1, keepdims=True)
    centered = token_rows - row_mean
    variance = jnp.mean(centered * centered, axis=1, keepdims=True)
    normed = (centered * lax.rsqrt(variance + norm_eps)).astype(jnp.bfloat16)
    route_ids = expert_ids.reshape(-1, 2)
    route_mix = expert_mix.reshape(-1, 2)
    expert_iota = jnp.arange(gate_serve.shape[0], dtype=jnp.int32)
    expert_gates = jnp.sum(
        (route_ids[:, :, None] == expert_iota[None, None, :]).astype(jnp.float32)
        * route_mix[:, :, None],
        axis=1,
    )
    gate_act = jnp.einsum("rd,edf->ref", normed, gate_serve, preferred_element_type=jnp.float32)
    up_act = jnp.einsum("rd,edf->ref", normed, up_serve, preferred_element_type=jnp.float32)
    hidden = (jax.nn.silu(gate_act) * up_act * expert_gates[:, :, None]).astype(jnp.bfloat16)
    part = jnp.einsum("ref,edf->rd", hidden, down_serve, preferred_element_type=jnp.float32)
    mixed = summed_rows(part.astype(jnp.bfloat16)).reshape(12, 1, width)
    return (gate_serve, up_serve, down_serve, mixed)


def solution(mesh):
    finer = Mesh(mesh.devices.reshape(NZ, NX, NC, mesh.shape["tp"]), ("fs_0", "fs_1", "fs_2", "tp"))
    placed = (
        P(None, "tp", None),
        P(FS),
        P(None, FS, "tp"),
        P(None, FS, "tp"),
        P(None, FS, "tp"),
        P(None, "tp", None),
        P(None, "tp", None),
    )
    return jax.shard_map(
        local,
        mesh=finer,
        in_specs=placed,
        out_specs=(P(None, None, FS), P(None, None, FS), P(None, None, FS), P(FS, "tp", None)),
        check_vma=False,
    )
```

time: 327 us -> 152 us (0.46)
  waiting for transfers between devices: 162 us -> 0 us
  Pallas kernels: 0 us -> 134 us
  blocking collectives: 83.3 us -> 0 us
  local copies, waits for them, and re-layouts: 49.5 us -> 6.57 us
  between operations: 14.6 us -> 0.76 us
    pallas_call x0 -> x2, Pallas kernels: none -> 134 us  [the longest x1 97.8 us: handed_over(): pl.pallas_call(weights_kernel, out_shape=(out, out, out), in_specs=[pl.Bl...]
    reduce_scatter x2 -> x0, waiting for transfers between devices: 100 us -> none  [summed_rows(): so_far = lax.psum_scatter(so_far, axis, scatter_dimension=0, tiled=True)]
    all_to_all x2 -> x0, blocking collectives: 76.8 us -> none  [sent_together(): lax.all_to_all(both, axis, split_axis=split_dim, concat_axis=concat_dim,...]
    all_gather x1 -> x0, waiting for transfers between devices: 61.6 us -> none  [sent_together_2(): lax.all_gather(both, axis, axis=dim, tiled=True)]
    unnamed x21 -> x18, local copies, waits for them, and re-layouts: 19.3 us -> 5.89 us
    concatenate x2 -> x0, local copies, waits for them, and re-layouts: 11.8 us -> none  [the longest x1 7.33 us: sent_together(): both = jnp.concatenate(arrays, axis=along)]
    all_to_all x3 -> x0, local copies, waits for them, and re-layouts: 11 us -> none  [sent_together(): lax.all_to_all(both, axis, split_axis=split_dim, concat_axis=concat_dim,...]
    unnamed x1 -> x0, blocking collectives: 6.48 us -> none
  transfers between devices with their start and end apart: 4 -> 0, of which waited for: 4 -> 0; matrix products, arithmetic and copies ran while one was open for 1% -> 0% of each run, Pallas kernels for 0% -> 0%
where the time goes in v1:
time: 152 us
  Pallas kernels  134 us (88%)
  matrix products  7.43 us (5%)
  local copies, waits for them, and re-layouts  6.57 us (4%)
  other arithmetic  3.49 us (2%)
    pallas_call x1, Pallas kernels, handed_over(): pl.pallas_call(weights_kernel, out_shape=(out, out, out), in_specs=[pl.Bl...  97.8 us
    pallas_call x1, Pallas kernels, summed_rows(): pl.pallas_call(sum_kernel, out_shape=jax.ShapeDtypeStruct((12, 2048), bf1...  35.9 us
    unnamed x18, local copies, waits for them, and re-layouts  5.89 us
    unnamed x2, matrix products  5.55 us

profile of v1, /device:TPU:1, one launch (start us, length us, event | category | flops | bytes accessed | tf_op | source)
XLA Modules:
  0.0 151.9 jit_solution(13479571677038548839)
XLA Ops:
  0.6 0.0 copy-start
  0.6 2.5 %convert_reduce_fusion = f32[768]{0:T(1024)S(1)} fusion(bf16[768,1,2048]{2,0,1:T(8,128)(2,1)} %param.7), kind=kLoop, calls=%fused_computation | loop fusion | flops 3144960 | bytes 3148800 | tf_op jit(solution)/shard_map/reduce_sum | solution.py:374
  3.2 0.0 copy-start.6
  3.2 0.0 copy-start.4
  3.2 0.0 copy-start.5
  3.2 0.3 copy-done
  3.5 1.0 fusion.3
  4.4 0.0 copy-done.6
  4.4 0.7 broadcast_in_dim.2.gain_ref
  5.1 0.0 copy-done.4
  5.1 0.0 copy-done.5
  5.1 97.8 %weights.1 = (bf16[4,128,2048]{2,1,0:T(8,128)(2,1)}, bf16[4,128,2048]{2,1,0:T(8,128)(2,1)}, bf16[4,128,2048]{2,1,0:T(8,128)(2,1)}) custom-call(f32[32,128]{1,0:T(8,128)} %broadcast_in_dim.2.gain_ref, f32[8,32,1024]{2,1,0:T(8,128)} %gate_hbm.1, f32[8,32,1024]{2,1,0:T(8,128)} %up_hbm.1, f32[8,32,1024]{2,1,0:T(8,128)} %down_hbm.1), custom_call_target="tpu_custom_call" | custom-call | tf_op jit(solution)/shard_map/weights/pallas_call | solution.py:225
  102.9 0.0 copy-start.3
  102.9 3.6 %fusion.8 = f32[768,512]{0,1:S(1)} fusion(bf16[2048,512]{0,1:T(8,128)(2,1)} %bitcast.46, bf16[768,1,2048]{2,0,1:T(8,128)(2,1)S(1)} %copy-done, f32[768]{0:T(1024)S(1)} %add_rsqrt_fusion, f32[768]{0:T(1024)S(1)} %broadcast_multiply_fusion), kind=kOutput, calls=%fused_computation.16 | convolution fusion | flops 1616904192 | bytes 6821888
  106.6 0.0 copy-done.3
  106.6 1.9 %fusion.10 = f32[768,512]{0,1:S(1)} fusion(bf16[2048,512]{0,1:T(8,128)(2,1)S(1)} %bitcast.48, bf16[768,1,2048]{2,0,1:T(8,128)(2,1)S(1)} %copy-done, f32[768]{0:T(1024)S(1)} %add_rsqrt_fusion, f32[768]{0:T(1024)S(1)} %broadcast_multiply_fusion), kind=kOutput, calls=%fused_computation.17 | convolution fusion | flops 1616904192 | bytes 6821888
  108.5 0.0 copy-done.1
  108.5 1.9 %bitcast_convert_fusion = bf16[768,2048]{1,0:T(8,128)(2,1)S(1)} fusion(bf16[8,2048,64]{1,2,0:T(8,128)(2,1)S(1)} %bitcast.44, f32[768,8,64]{0,2,1:T(8,128)S(1)} %bitcast.52, f32[768,8,64]{0,2,1:T(8,128)S(1)} %bitcast.53, f32[768,8]{0,1:T(8,128)S(1)} %select_reduce_fusion), kind=kOutput, calls=%fused_computation.7 | convolution fusion | flops 1614938112 | bytes 8413184 | tf_op jit(solution)/shard_map/ref,edf->rd/dot_general | solution.py:389
  110.4 35.9 %sums.1 = bf16[12,2048]{1,0:T(8,128)(2,1)S(1)} custom-call(bf16[8,4,24,2048]{3,2,1,0:T(8,128)(2,1)S(1)} %bitcast.42), custom_call_target="tpu_custom_call" | custom-call | tf_op jit(solution)/shard_map/sums/pallas_call | solution.py:344
  146.3 1.3 copy.17
  147.6 1.0 copy-done.2
  148.6 1.3 copy.18
  150.0 1.3 copy.19
  151.3 0.6 copy.20
  (5 shorter events, 0.0 us)
Async XLA Ops:
  0.6 2.8 %copy-start = (bf16[768,1,2048]{2,0,1:T(8,128)(2,1)S(1)}, bf16[768,1,2048]{2,0,1:T(8,128)(2,1)}, u32[]{:S(2)}) copy-start(bf16[768,1,2048]{2,0,1:T(8,128)(2,1)} %param.7) | copy-start | bytes 9437188
  3.2 1.3 copy-start.6
  3.2 1.9 %copy-start.4 = (f32[768,1,2]{0,2,1:T(2,128)S(1)}, f32[768,1,2]{0,2,1:T(2,128)}, u32[]{:S(2)}) copy-start(f32[768,1,2]{0,2,1:T(2,128)} %param.13) | copy-start | bytes 18436
  3.2 1.9 %copy-start.5 = (s32[768,1,2]{0,2,1:T(2,128)S(1)}, s32[768,1,2]{0,2,1:T(2,128)}, u32[]{:S(2)}) copy-start(s32[768,1,2]{0,2,1:T(2,128)} %param.12) | copy-start | bytes 18436
  102.9 3.7 %copy-start.3 = (bf16[4,128,2048]{2,1,0:T(8,128)(2,1)S(1)}, bf16[4,128,2048]{2,1,0:T(8,128)(2,1)}, u32[]{:S(2)}) copy-start(bf16[4,128,2048]{2,1,0:T(8,128)(2,1)} %get-tuple-element.7) | copy-start | bytes 6291460
  106.6 1.9 %copy-start.1 = (bf16[4,128,2048]{2,1,0:T(8,128)(2,1)S(1)}, bf16[4,128,2048]{2,1,0:T(8,128)(2,1)}, u32[]{:S(2)}) copy-start(bf16[4,128,2048]{2,1,0:T(8,128)(2,1)} %get-tuple-element.9) | copy-start | bytes 6291460
  146.3 2.3 %copy-start.2 = (bf16[4,128,2048]{2,1,0:T(8,128)(2,1)S(1)}, bf16[4,128,2048]{2,1,0:T(8,128)(2,1)}, u32[]{:S(2)}) copy-start(bf16[4,128,2048]{2,1,0:T(8,128)(2,1)} %get-tuple-element.8) | copy-start | bytes 6291460

commit v2 on v0

v2 whole, which is shorter than its diff:
```python
import functools

import jax
import jax.numpy as jnp
from jax import lax
from jax.experimental import pallas as pl
from jax.experimental.pallas import tpu as pltpu
from jax.sharding import Mesh
from jax.sharding import PartitionSpec as P

FS = ("fs_0", "fs_1", "fs_2")
NZ, NX, NC, NY = 8, 4, 2, 4
NXC = NX * NC
MESH = pl.DeviceIdType.MESH


NH, NQ = 2, 4
HR = 32 // NH
QC = 2048 // NQ

norm_eps = 1e-05


def remote(src, dst, send, recv, **where):
    return pltpu.make_async_remote_copy(
        src_ref=src, dst_ref=dst, send_sem=send, recv_sem=recv, device_id=where, device_id_type=MESH
    )


def layer_kernel(
    tok_hbm, gain_ref, gate_hbm, up_hbm, down_hbm, ids_ref, mix_ref,
    gate_out, up_out, down_out, mixed_ref,
    win, packed, by_plane, by_z, rows, turned, normed, square, route, hidden,
    part, pair_in, chip, x_in, mine, z_in, piece, other,
    in_sem, out_sem, y_send, y_recv, z_send, z_recv, x_send, x_recv, g_send, g_recv,
    d_send, d_recv, p_send, p_recv, s_send, s_recv, t_send, t_recv, o_send, o_recv,
):
    z, x, c, y = (lax.axis_index(a) for a in ("fs_0", "fs_1", "fs_2", "tp"))
    xc = x * NC + c
    f32, bf16 = jnp.float32, jnp.bfloat16
    loads = [
        pltpu.make_async_copy(ref, win.at[w], in_sem.at[w])
        for w, ref in enumerate((gate_hbm, up_hbm, down_hbm))
    ]
    loads.append(pltpu.make_async_copy(tok_hbm, normed, in_sem.at[3]))
    for load in loads:
        load.start()

    def z_of(j):
        return lax.rem(z + j, NZ)

    def y_of(j):
        return lax.rem(y + j, NY)

    def x_of(j):
        return lax.rem(x + j, NX)

    def xc_of(j):
        to = lax.rem(xc + j, NXC)
        return to, {"fs_1": lax.div(to, NC), "fs_2": lax.rem(to, NC)}

    sent = []

    def go(copies):
        for copy in copies:
            copy.start()
            sent.append(copy)
        return copies

    def wait(copies):
        for copy in copies:
            copy.wait_recv()

    left_lanes = lax.broadcasted_iota(jnp.int32, (32, 128), 1) < 64
    left_half = lax.broadcasted_iota(jnp.int32, (1, 128), 1) < 64

    square[...] = jnp.zeros_like(square)
    square[:, :32] = jnp.broadcast_to(gain_ref[...], (128, 32))
    gain = square[...].T[:32]
    square[:32] = gain

    def fold(w):
        loads[w].wait()

        def block(j, carry):
            at = pl.ds(pl.multiple_of(j * 128, 128), 128)
            for g in range(NY):
                one = win[w, 2 * g, :, at]
                two = win[w, 2 * g + 1, :, at]
                if w < 2:
                    one, two = one * square[:32], two * square[:32]
                first = jnp.where(left_lanes, one, pltpu.roll(two, 64, 1))
                second = jnp.where(left_lanes, pltpu.roll(one, 64, 1), two)
                packed[w, g, 2 * j] = first.astype(bf16)
                packed[w, g, 2 * j + 1] = second.astype(bf16)
            return carry

        lax.fori_loop(0, 8, block, 0)

    def part_of(h):
        return pl.ds(h * HR, HR)

    def y_copies(w, h):
        return [
            remote(
                packed.at[w, y_of(j), :, part_of(h)], by_plane.at[w, y, :, part_of(h)],
                y_send.at[w, h, j - 1], y_recv.at[w, h, j - 1], tp=y_of(j),
            )
            for j in (1, 3, 2)
        ]

    def z_copies(w, h):
        copies = []
        for j in (1, 7, 2, 6, 3, 5, 4):
            to = z_of(j)
            half = lax.rem(to, 2) * 8
            copies.append(
                remote(
                    by_plane.at[w, lax.div(to, 2), pl.ds(half, 8), part_of(h)],
                    by_z.at[w, z, :, part_of(h)],
                    z_send.at[w, h, j - 1], z_recv.at[w, h, j - 1], fs_0=to,
                )
            )
        return copies

    def x_copies(w, h):
        copies = []
        for j in range(1, NXC):
            to, where = xc_of(j)
            copies.append(
                remote(
                    by_z.at[w, :, to, part_of(h)], rows.at[w, y, :, xc, part_of(h)],
                    x_send.at[w, h, j - 1], x_recv.at[w, h, j - 1], **where,
                )
            )
        return copies

    def g_copies(w, h):
        own = rows.at[w, y, :, :, part_of(h)]
        return [
            remote(own, own, g_send.at[w, h, 0], g_recv.at[w, h, 0], tp=y_of(1)),
            remote(own, own, g_send.at[w, h, 1], g_recv.at[w, h, 1], tp=y_of(3)),
        ]

    def f_copies(w, h):
        lo = rows.at[w, y_of(3), pl.ds(0, 4), :, part_of(h)]
        hi = rows.at[w, y_of(1), pl.ds(4, 4), :, part_of(h)]
        return [
            remote(lo, lo, g_send.at[w, h, 2], g_recv.at[w, h, 2], tp=y_of(1)),
            remote(hi, hi, g_send.at[w, h, 3], g_recv.at[w, h, 3], tp=y_of(3)),
        ]

    QZ = NZ // NQ

    def dg_copies(q):
        own = rows.at[2, y, pl.ds(q * QZ, QZ)]
        return [
            remote(own, own, d_send.at[q, 0], d_recv.at[q, 0], tp=y_of(1)),
            remote(own, own, d_send.at[q, 1], d_recv.at[q, 1], tp=y_of(3)),
        ]

    def df_copies(q):
        lo = rows.at[2, y_of(3), pl.ds(q * QZ, QZ // 2)]
        hi = rows.at[2, y_of(1), pl.ds(q * QZ + QZ // 2, QZ // 2)]
        return [
            remote(lo, lo, d_send.at[q, 2], d_recv.at[q, 2], tp=y_of(1)),
            remote(hi, hi, d_send.at[q, 3], d_recv.at[q, 3], tp=y_of(3)),
        ]

    ys, zs, xs, gs, fs = ({} for _ in range(5))
    dg, df, pairs, sums, tops, ends = ({} for _ in range(6))

    def start_y(w, h):
        ys[w, h] = go(y_copies(w, h))
        by_plane[w, y, :, part_of(h)] = packed[w, y, :, part_of(h)]

    def start_z(w, h):
        wait(ys[w, h])
        zs[w, h] = go(z_copies(w, h))
        half = pl.ds(lax.rem(z, 2) * 8, 8)
        by_z[w, z, :, part_of(h)] = by_plane[w, lax.div(z, 2), half, part_of(h)]

    def start_x(w, h):
        wait(zs[w, h])
        xs[w, h] = go(x_copies(w, h))
        rows[w, y, :, xc, part_of(h)] = by_z[w, :, xc, part_of(h)]

    def start_g(w, h):
        wait(xs[w, h])
        gs[w, h] = go(g_copies(w, h))

    def start_f(w, h):
        wait(gs[w, h])
        fs[w, h] = go(f_copies(w, h))

    def start_dg(q):
        dg[q] = go(dg_copies(q))

    def start_df(q):
        wait(dg[q])
        df[q] = go(df_copies(q))

    def spread(i, carry):
        at = pl.ds(pl.multiple_of(i * 128, 128), 128)
        for k in range(2):
            wide = jnp.broadcast_to(ids_ref[k : k + 1, at].astype(f32), (128, 128))
            route[k, at] = wide.T
            wide = jnp.broadcast_to(mix_ref[k : k + 1, at], (128, 128))
            route[2 + k, at] = wide.T
        return carry

    def normalize(start, stop):
        def block(i, carry):
            at = pl.ds(pl.multiple_of(i * 64, 64), 64)
            values = normed[at].astype(f32)
            centered = values - jnp.mean(values, axis=1, keepdims=True)
            variance = jnp.mean(centered * centered, axis=1, keepdims=True)
            normed[at] = (centered * lax.rsqrt(variance + norm_eps)).astype(bf16)
            return carry

        lax.fori_loop(start, stop, block, 0)

    def turn(w, g):
        def block(i, carry):
            for k in range(2):
                tile = rows[w, g, 2 * i + k].reshape(256, 128).astype(f32).T.astype(bf16)
                at = pl.ds(pl.multiple_of(i * 512 + k * 256, 256), 256)
                turned[w, g, :, at] = tile
            return carry

        lax.fori_loop(0, 4, block, 0)

    outs = (gate_out, up_out, down_out)
    stores = []

    def store(w):
        copy = pltpu.make_async_copy(turned.at[w], outs[w], out_sem.at[w])
        copy.start()
        stores.append(copy)

    def hidden_of(g):
        both = jnp.concatenate(
            [rows[0, g].reshape(2048, 128), rows[1, g].reshape(2048, 128)], axis=1
        )
        expert = jnp.where(left_half, 2 * g, 2 * g + 1).astype(f32)

        def block(i, carry):
            at = pl.ds(pl.multiple_of(i * 256, 256), 256)
            acts = jnp.dot(normed[at], both, preferred_element_type=f32)
            gate_act, up_act = acts[:, :128], acts[:, 128:]
            weight = jnp.where(route[0, at] == expert, route[2, at], 0.0)
            weight = weight + jnp.where(route[1, at] == expert, route[3, at], 0.0)
            value = gate_act / (1.0 + jnp.exp(-gate_act)) * up_act * weight
            hidden[at, pl.ds(pl.multiple_of(g * 128, 128), 128)] = value.astype(bf16)
            return carry

        lax.fori_loop(0, 3, block, 0)

    def columns(of):
        return pl.ds(pl.multiple_of(of * (QC // 2), 128), QC // 2)

    def partial_of(q):
        wait(df[q])
        down = jnp.concatenate(
            [rows[2, g, pl.ds(q * QZ, QZ)].reshape(QC, 128) for g in range(NY)], axis=1
        )

        def block(i, carry):
            at = pl.ds(pl.multiple_of(i * 384, 384), 384)
            value = lax.dot_general(
                hidden[at], down, (((1,), (1,)), ((), ())), preferred_element_type=f32
            )
            part[q, pl.ds(i * 4, 4)] = value.reshape(4, NX, 24, QC).astype(bf16)
            return carry

        lax.fori_loop(0, 2, block, 0)
        pairs[q] = go(
            [remote(part.at[q, :, :, :, columns(1 - c)], pair_in.at[q], p_send.at[q], p_recv.at[q], fs_2=1 - c)]
        )

    def start_sums(q):
        wait(pairs[q])

        def add(i, carry):
            for j in range(NX):
                own = part[q, i, j, :, columns(c)].astype(f32)
                chip[q, j, i] = (own + pair_in[q, i, j].astype(f32)).astype(bf16)
            return carry

        lax.fori_loop(0, NZ, add, 0)
        sums[q] = go(
            [
                remote(chip.at[q, x_of(j)], x_in.at[q, j - 1], s_send.at[q, j - 1], s_recv.at[q, j - 1], fs_1=x_of(j))
                for j in (1, 3, 2)
            ]
        )

    def start_tops(q):
        wait(sums[q])

        def add(i, carry):
            value = chip[q, x, i].astype(f32)
            for j in range(3):
                value = value + x_in[q, j, i].astype(f32)
            mine[q, i] = value.astype(bf16)
            return carry

        lax.fori_loop(0, NZ, add, 0)
        tops[q] = go(
            [
                remote(mine.at[q, z_of(j)], z_in.at[q, j - 1], t_send.at[q, j - 1], t_recv.at[q, j - 1], fs_0=z_of(j))
                for j in (4, 3, 5, 2, 6, 1, 7)
            ]
        )

    def start_ends(q):
        wait(tops[q])
        total = mine[q, z].astype(f32)
        for j in range(7):
            total = total + z_in[q, j].astype(f32)
        piece[q] = total.astype(bf16)
        ends[q] = go([remote(piece.at[q], other.at[q], o_send.at[q], o_recv.at[q], fs_2=1 - c)])

    def finish(q):
        wait(ends[q])
        here, there = piece[q].astype(f32), other[q].astype(f32)
        here = jnp.where(c == 0, here[:12], here[12:])
        there = jnp.where(c == 0, there[:12], there[12:])
        wide = QC // 2
        mixed_ref[:, q * QC : q * QC + wide] = jnp.where(c == 0, here, there).astype(bf16)
        mixed_ref[:, q * QC + wide : (q + 1) * QC] = jnp.where(c == 0, there, here).astype(bf16)

    barrier = pltpu.get_barrier_semaphore()
    peers = (
        [{"tp": y_of(j)} for j in range(1, NY)]
        + [{"fs_0": z_of(j)} for j in range(1, NZ)]
        + [xc_of(j)[1] for j in range(1, NXC)]
    )
    for where in peers:
        pl.semaphore_signal(barrier, inc=1, device_id=where, device_id_type=MESH)
    fold(0)
    pl.semaphore_wait(barrier, len(peers))

    start_y(0, 0)
    start_y(0, 1)
    fold(1)
    start_y(1, 0)
    start_y(1, 1)
    fold(2)
    start_y(2, 0)
    start_y(2, 1)
    start_z(0, 0)
    lax.fori_loop(0, 6, spread, 0)
    loads[3].wait()
    start_z(0, 1)
    normalize(0, 4)
    start_z(1, 0)
    normalize(4, 8)
    start_z(1, 1)
    normalize(8, 12)
    start_x(0, 0)
    start_z(2, 0)
    start_z(2, 1)
    start_g(0, 0)
    start_x(0, 1)
    start_g(0, 1)
    start_x(1, 0)
    turn(0, y)
    start_f(0, 0)
    start_g(1, 0)
    start_x(1, 1)
    start_f(0, 1)
    start_g(1, 1)
    start_x(2, 0)
    turn(1, y)
    turn(0, y_of(1))
    start_f(1, 0)
    turn(0, y_of(3))
    start_x(2, 1)
    hidden_of(y)
    wait(fs[0, 0])
    wait(fs[0, 1])
    wait(xs[2, 0])
    wait(xs[2, 1])
    start_dg(0)
    start_f(1, 1)
    start_dg(1)
    hidden_of(y_of(1))
    start_df(0)
    start_dg(2)
    hidden_of(y_of(3))
    start_df(1)
    start_dg(3)
    turn(0, y_of(2))
    store(0)
    wait(fs[1, 0])
    wait(fs[1, 1])
    hidden_of(y_of(2))
    start_df(2)
    partial_of(0)
    turn(1, y_of(1))
    start_df(3)
    partial_of(1)
    start_sums(0)
    turn(1, y_of(3))
    turn(1, y_of(2))
    store(1)
    partial_of(2)
    start_sums(1)
    start_tops(0)
    partial_of(3)
    start_sums(2)
    start_tops(1)
    start_ends(0)
    turn(2, y)
    turn(2, y_of(1))
    start_sums(3)
    start_tops(2)
    start_ends(1)
    turn(2, y_of(3))
    turn(2, y_of(2))
    store(2)
    start_tops(3)
    start_ends(2)
    finish(0)
    finish(1)
    start_ends(3)
    finish(2)
    finish(3)
    for copy in sent:
        copy.wait_send()
    for copy in stores:
        copy.wait()


def local(tokens, norm_gain, gate_weight, up_weight, down_weight, expert_ids, expert_mix):
    f32, bf16, dma = jnp.float32, jnp.bfloat16, pltpu.SemaphoreType.DMA
    out = jax.ShapeDtypeStruct((NY, 128, 2048), bf16)
    anywhere = pl.BlockSpec(memory_space=pl.ANY)
    vmem = pl.BlockSpec(memory_space=pltpu.VMEM)
    wide = QC // 2

    def both(*shape):
        return [dma(shape), dma(shape)]

    gate_serve, up_serve, down_serve, mixed = pl.pallas_call(
        layer_kernel,
        out_shape=(out, out, out, jax.ShapeDtypeStruct((12, 2048), bf16)),
        in_specs=[anywhere, vmem, anywhere, anywhere, anywhere, vmem, vmem],
        out_specs=(anywhere, anywhere, anywhere, vmem),
        scratch_shapes=[
            pltpu.VMEM((3, 8, 32, 1024), f32),
            pltpu.VMEM((3, NY, 16, 32, 128), bf16),
            pltpu.VMEM((3, NY, 16, 32, 128), bf16),
            pltpu.VMEM((3, NZ, NXC, 32, 128), bf16),
            pltpu.VMEM((3, NY, NZ, NXC, 32, 128), bf16),
            pltpu.VMEM((3, NY, 128, 2048), bf16),
            pltpu.VMEM((768, 2048), bf16),
            pltpu.VMEM((128, 128), f32),
            pltpu.VMEM((4, 768, 128), f32),
            pltpu.VMEM((768, 512), bf16),
            pltpu.VMEM((NQ, NZ, NX, 24, QC), bf16),
            pltpu.VMEM((NQ, NZ, NX, 24, wide), bf16),
            pltpu.VMEM((NQ, NX, NZ, 24, wide), bf16),
            pltpu.VMEM((NQ, 3, NZ, 24, wide), bf16),
            pltpu.VMEM((NQ, NZ, 24, wide), bf16),
            pltpu.VMEM((NQ, 7, 24, wide), bf16),
            pltpu.VMEM((NQ, 24, wide), bf16),
            pltpu.VMEM((NQ, 24, wide), bf16),
            dma((4,)), dma((3,)),
            *both(3, NH, 3), *both(3, NH, 7), *both(3, NH, 7), *both(2, NH, 4),
            *both(NQ, 4), *both(NQ), *both(NQ, 3), *both(NQ, 7), *both(NQ),
        ],
        compiler_params=pltpu.CompilerParams(
            collective_id=0, has_side_effects=True, vmem_limit_bytes=56 * 2**20
        ),
        name="layer",
    )(
        tokens.reshape(768, 2048), norm_gain.reshape(1, 32), gate_weight, up_weight, down_weight,
        expert_ids.reshape(768, 2).T, expert_mix.reshape(768, 2).T,
    )
    gate_serve, up_serve, down_serve = (
        jnp.swapaxes(a.reshape(8, 64, 2048), 1, 2) for a in (gate_serve, up_serve, down_serve)
    )
    return (gate_serve, up_serve, down_serve, mixed.reshape(12, 1, 2048))


def solution(mesh):
    finer = Mesh(mesh.devices.reshape(NZ, NX, NC, mesh.shape["tp"]), ("fs_0", "fs_1", "fs_2", "tp"))
    placed = (
        P(None, "tp", None),
        P(FS),
        P(None, FS, "tp"),
        P(None, FS, "tp"),
        P(None, FS, "tp"),
        P(None, "tp", None),
        P(None, "tp", None),
    )
    return jax.shard_map(
        local,
        mesh=finer,
        in_specs=placed,
        out_specs=(P(None, None, FS), P(None, None, FS), P(None, None, FS), P(FS, "tp", None)),
        check_vma=False,
    )
```

time: 327 us -> 121 us (0.37)
  waiting for transfers between devices: 162 us -> 0 us
  Pallas kernels: 0 us -> 113 us
  blocking collectives: 83.3 us -> 0 us
  local copies, waits for them, and re-layouts: 49.5 us -> 7.61 us
  between operations: 14.6 us -> 0.65 us
  matrix products: 8.38 us -> 0 us
  other arithmetic: 6.63 us -> 0 us
    pallas_call x0 -> x1, Pallas kernels: none -> 113 us  [local(): pl.pallas_call(layer_kernel, out_shape=(out, out, out, jax.ShapeDtypeStru...]
    reduce_scatter x2 -> x0, waiting for transfers between devices: 100 us -> none  [summed_rows(): so_far = lax.psum_scatter(so_far, axis, scatter_dimension=0, tiled=True)]
    all_to_all x2 -> x0, blocking collectives: 76.8 us -> none  [sent_together(): lax.all_to_all(both, axis, split_axis=split_dim, concat_axis=concat_dim,...]
    all_gather x1 -> x0, waiting for transfers between devices: 61.6 us -> none  [sent_together_2(): lax.all_gather(both, axis, axis=dim, tiled=True)]
    concatenate x2 -> x0, local copies, waits for them, and re-layouts: 11.8 us -> none  [the longest x1 7.33 us: sent_together(): both = jnp.concatenate(arrays, axis=along)]
    unnamed x21 -> x10, local copies, waits for them, and re-layouts: 19.3 us -> 7.61 us
    all_to_all x3 -> x0, local copies, waits for them, and re-layouts: 11 us -> none  [sent_together(): lax.all_to_all(both, axis, split_axis=split_dim, concat_axis=concat_dim,...]
    unnamed x1 -> x0, blocking collectives: 6.48 us -> none
  transfers between devices with their start and end apart: 4 -> 0, of which waited for: 4 -> 0; matrix products, arithmetic and copies ran while one was open for 1% -> 0% of each run, Pallas kernels for 0% -> 0%
where the time goes in v2:
time: 121 us
  Pallas kernels  113 us (93%)
  local copies, waits for them, and re-layouts  7.61 us (6%)
    pallas_call x1, Pallas kernels, local(): pl.pallas_call(layer_kernel, out_shape=(out, out, out, jax.ShapeDtypeStru...  113 us
    unnamed x10, local copies, waits for them, and re-layouts  7.61 us

profile of v2, /device:TPU:1, one launch (start us, length us, event | category | flops | bytes accessed | tf_op | source)
XLA Modules:
  0.0 121.2 jit_solution(14055703534724298557)
XLA Ops:
  0.6 113.0 %layer.1 = (bf16[4,128,2048]{2,1,0:T(8,128)(2,1)}, bf16[4,128,2048]{2,1,0:T(8,128)(2,1)}, bf16[4,128,2048]{2,1,0:T(8,128)(2,1)}, bf16[12,2048]{1,0:T(8,128)(2,1)}) custom-call(bf16[768,2048]{1,0:T(8,128)(2,1)} %bitcast.18, f32[1,32]{1,0:T(1,128)} %bitcast.25, f32[8,32,1024]{2,1,0:T(8,128)} %gate_hbm.1, f32[8,32,1024]{2,1,0:T(8,128)} %up_hbm.1, ...), custom_call_target="tpu_custom_call" | custom-call | tf_op jit(solution)/shard_map/layer/pallas_call | solution.py:446
  113.6 0.0 copy-start.1
  113.6 3.3 %copy.15 = bf16[8,2048,64]{1,2,0:T(8,128)(2,1)} copy(bf16[8,2048,64]{1,2,0:T(8,128)(2,1)} %bitcast.21) | data formatting | bytes 4194304
  116.9 0.0 copy-done.1
  116.9 0.0 copy-start
  116.9 1.3 %copy.16 = bf16[8,2048,64]{1,2,0:T(8,128)(2,1)} copy(bf16[8,2048,64]{1,2,0:T(8,128)(2,1)S(1)} %bitcast.20) | data formatting | bytes 4194304
  118.2 1.0 copy-done
  119.3 0.0 copy-start.2
  119.3 1.3 %copy.17 = bf16[8,2048,64]{1,2,0:T(8,128)(2,1)} copy(bf16[8,2048,64]{1,2,0:T(8,128)(2,1)S(1)} %bitcast.19) | data formatting | bytes 4194304
  120.6 0.0 copy-done.2
  120.6 0.6 copy.18
Async XLA Ops:
  113.6 3.3 %copy-start.1 = (bf16[4,128,2048]{2,1,0:T(8,128)(2,1)S(1)}, bf16[4,128,2048]{2,1,0:T(8,128)(2,1)}, u32[]{:S(2)}) copy-start(bf16[4,128,2048]{2,1,0:T(8,128)(2,1)} %get-tuple-element.9) | copy-start | bytes 6291460
  116.9 2.3 %copy-start = (bf16[4,128,2048]{2,1,0:T(8,128)(2,1)S(1)}, bf16[4,128,2048]{2,1,0:T(8,128)(2,1)}, u32[]{:S(2)}) copy-start(bf16[4,128,2048]{2,1,0:T(8,128)(2,1)} %get-tuple-element.10) | copy-start | bytes 6291460
  119.3 1.3 %copy-start.2 = (bf16[12,2048]{1,0:T(8,128)(2,1)S(1)}, bf16[12,2048]{1,0:T(8,128)(2,1)}, u32[]{:S(2)}) copy-start(bf16[12,2048]{1,0:T(8,128)(2,1)} %get-tuple-element.11) | copy-start | bytes 147460
